TPU v7x, 32 devices: a whole 2x2x4 slice. The times are simulated.
32 devices in a mesh: ep: 16 (over z, y, x), tp: 2 (over core).
Axes of the slice: x: 2, y: 2, z: 4, core: 2. Of those that a mesh axis runs over, the one named last changes fastest.
Arguments:
- stream: bfloat16 [512, 2048], P('ep'), may hold values from -6 to 6
- mixer_gain: float32 [2048], replicated, may hold values from 0.1 to 1.9
- gate_proj: bfloat16 [2048, 1024], P(None, 'tp'), may hold values from -0.125 to 0.125
- input_proj: bfloat16 [2048, 1024], P(None, 'tp'), may hold values from -0.125 to 0.125
- state_maps: bfloat16 [2, 2048, 256], P(None, None, 'tp'), may hold values from -0.125 to 0.125
- step_proj: bfloat16 [2048, 16], P(None, 'tp'), may hold values from -0.125 to 0.125
- step_bias: float32 [16], P('tp'), may hold values from -3 to 0.5
- decay_rate: float32 [16], P('tp'), may hold values from 0.05 to 4
- input_taps: float32 [4, 1024], P(None, 'tp'), may hold values from -3 to 3
- map_taps: float32 [2, 4, 256], P(None, None, 'tp'), may hold values from -3 to 3
- input_past: bfloat16 [512, 3, 1024], P('ep', None, 'tp'), may hold values from -6 to 6
- map_past: bfloat16 [512, 2, 3, 256], P('ep', None, None, 'tp'), may hold values from -6 to 6
- head_state: float32 [512, 16, 4096], P('ep', 'tp'), may hold values from -1.6 to 1.6
- skip_gain: float32 [16], P('tp'), may hold values from 0 to 2
- inner_gain: float32 [1024], P('tp'), may hold values from 0.1 to 1.9
- mixer_out: bfloat16 [1024, 2048], P('tp'), may hold values from -0.1875 to 0.1875
- channel_gain: float32 [2048], replicated, may hold values from 0.1 to 1.9
- expert_ids: int32 [512, 2], P('ep'), may hold values from 0 to 7, all different within a row; in each aligned block of 32 rows (0 to 31, 32 to 63, ...) at most 12 rows name the same one
- expert_weight: float32 [512, 2], P('ep'), may hold values from 0.2 to 1
- expert_gate: bfloat16 [2048, 57344], P(None, ('ep', 'tp')), may hold values from -0.125 to 0.125
- expert_up: bfloat16 [2048, 57344], P(None, ('ep', 'tp')), may hold values from -0.125 to 0.125
- expert_down: bfloat16 [57344, 2048], P(('ep', 'tp')), may hold values from -0.0625 to 0.0625
- dense_gate: bfloat16 [2048, 5632], P('tp', 'ep'), may hold values from -0.125 to 0.125
- dense_up: bfloat16 [2048, 5632], P('tp', 'ep'), may hold values from -0.125 to 0.125
- dense_down: bfloat16 [5632, 2048], P('ep', 'tp'), may hold values from -0.078125 to 0.078125
- dense_mix: float32 [2048], P('tp'), may hold values from -2 to 2
Outputs:
- stream_out: bfloat16 [512, 2048], P('ep', 'tp')
- state_out: float32 [512, 16, 4096], P('ep', 'tp')
Inputs may be any that keep to these rules, and one draw needn't show every extreme that they name: `expert_ids`: each row names 2 different experts. In each aligned block of 32 rows no expert is named by more than 12 rows, and in some block one expert is named by exactly 12 rows.
All inputs are finite; a program needn't handle non-finite values.
Results may differ from a plain program's by a relative error of at most 0.015.
Values may be sent and summed in bfloat16 or wider, within the bound.
A program may use at most 128 MiB of HBM per device.

v0:
```python
import jax
import jax.numpy as jnp
from jax import lax
from jax.sharding import PartitionSpec as P

HEAD = 64
HEADS = 16
GROUPS = 4
NSTATE = 64
EXPERTS = 8
TOP_K = 2
CAP = 12
EPS = 1e-06


def rms_scale(values):
    return values * lax.rsqrt(jnp.mean(values * values, axis=-1, keepdims=True) + EPS)


def short_conv(past_rows, newest, tap_weights, along):
    window = jnp.concatenate([past_rows, jnp.expand_dims(newest, along)], axis=along).astype(
        jnp.float32
    )
    return jax.nn.silu(jnp.sum(window * tap_weights, axis=along))


def mix_heads(
    stream,
    mixer_gain,
    gate_proj,
    input_proj,
    state_maps,
    step_proj,
    step_bias,
    decay_rate,
    input_taps,
    map_taps,
    input_past,
    map_past,
    head_state,
    skip_gain,
    inner_gain,
):
    row_count = stream.shape[0]
    normed = (rms_scale(stream.astype(jnp.float32)) * mixer_gain).astype(jnp.bfloat16)
    gate_in = jnp.dot(normed, gate_proj, preferred_element_type=jnp.float32).astype(jnp.bfloat16)
    input_new = jnp.dot(normed, input_proj, preferred_element_type=jnp.float32).astype(jnp.bfloat16)
    map_new = jnp.stack(
        [
            jnp.dot(normed, state_maps[0], preferred_element_type=jnp.float32),
            jnp.dot(normed, state_maps[1], preferred_element_type=jnp.float32),
        ],
        axis=1,
    ).astype(jnp.bfloat16)
    step_size = jax.nn.softplus(
        jnp.dot(normed, step_proj, preferred_element_type=jnp.float32) + step_bias
    )
    conv_in = short_conv(input_past, input_new, input_taps, 1)
    conv_map = short_conv(map_past, map_new, map_taps, 2)
    head_count = step_size.shape[1]
    per_group = HEADS // GROUPS
    group_count = head_count // per_group
    write_map = jnp.repeat(
        conv_map[:, 0].reshape(row_count, group_count, NSTATE), per_group, axis=1
    )
    read_map = jnp.repeat(conv_map[:, 1].reshape(row_count, group_count, NSTATE), per_group, axis=1)
    values = conv_in.reshape(row_count, head_count, HEAD)
    decay_now = jnp.exp(-decay_rate * step_size)
    state_old = head_state.reshape(row_count, head_count, HEAD, NSTATE)
    state_new = (
        decay_now[:, :, None, None] * state_old
        + (step_size[:, :, None] * values)[:, :, :, None] * write_map[:, :, None, :]
    )
    gated = jnp.sum(state_new * read_map[:, :, None, :], axis=3) + skip_gain[:, None] * values
    gated = gated.reshape(row_count, head_count * HEAD) * jax.nn.silu(gate_in.astype(jnp.float32))
    inner_out = (
        rms_scale(gated.reshape(row_count, group_count, -1)).reshape(row_count, -1) * inner_gain
    )
    return (inner_out.astype(jnp.bfloat16), state_new.reshape(row_count, head_count, HEAD * NSTATE))


def local(
    stream,
    mixer_gain,
    gate_proj,
    input_proj,
    state_maps,
    step_proj,
    step_bias,
    decay_rate,
    input_taps,
    map_taps,
    input_past,
    map_past,
    head_state,
    skip_gain,
    inner_gain,
    mixer_out,
    channel_gain,
    expert_ids,
    expert_weight,
    expert_gate,
    expert_up,
    expert_down,
    dense_gate,
    dense_up,
    dense_down,
    dense_mix,
):
    inner_out, state_out = mix_heads(
        stream,
        mixer_gain,
        gate_proj,
        input_proj,
        state_maps,
        step_proj,
        step_bias,
        decay_rate,
        input_taps,
        map_taps,
        input_past,
        map_past,
        head_state,
        skip_gain,
        inner_gain,
    )
    partial_out = jnp.dot(inner_out, mixer_out, preferred_element_type=jnp.float32)
    mixed = lax.psum(partial_out.astype(jnp.bfloat16), "tp").astype(jnp.float32)
    hidden_mid = stream.astype(jnp.float32) + mixed
    ffn_in = (rms_scale(hidden_mid) * channel_gain).astype(jnp.bfloat16)
    row_count, feature_count = ffn_in.shape
    half_width = feature_count // lax.axis_size("tp")
    offset = lax.axis_index("tp") * half_width
    own_half = lax.dynamic_slice_in_dim(ffn_in, offset, half_width, 1)
    kept = lax.dynamic_slice_in_dim(hidden_mid, offset, half_width, 1)
    expert_span = lax.axis_size("ep") // EXPERTS
    flat_ids = expert_ids.reshape(-1)
    hit_table = (flat_ids[:, None] == jnp.arange(EXPERTS, dtype=jnp.int32)[None, :]).astype(
        jnp.int32
    )
    slot_rank = jnp.sum(jnp.cumsum(hit_table, axis=0) * hit_table, axis=1) - 1
    slot_index = flat_ids * CAP + slot_rank
    slot_table = (
        slot_index[:, None] == jnp.arange(EXPERTS * CAP, dtype=jnp.int32)[None, :]
    ).astype(jnp.float32)
    slot_table = slot_table.reshape(row_count, TOP_K, EXPERTS * CAP)
    chosen = jnp.sum(slot_table, axis=1).astype(jnp.bfloat16)
    outgoing = jnp.dot(chosen.T, ffn_in, preferred_element_type=jnp.float32).astype(jnp.bfloat16)
    outgoing = jnp.repeat(outgoing.reshape(EXPERTS, CAP, feature_count), expert_span, axis=0)
    received = lax.all_to_all(outgoing, "ep", split_axis=0, concat_axis=0, tiled=True)
    sources, item_count, width_in = received.shape
    flat_rows = received.reshape(sources * item_count, width_in)
    gate_val = jnp.dot(flat_rows, expert_gate, preferred_element_type=jnp.float32)
    up_val = jnp.dot(flat_rows, expert_up, preferred_element_type=jnp.float32)
    act = (jax.nn.silu(gate_val) * up_val).astype(jnp.bfloat16)
    share = jnp.dot(act, expert_down, preferred_element_type=jnp.float32).reshape(
        sources, item_count, width_in
    )
    halves = lax.psum_scatter(
        share.astype(jnp.bfloat16), "tp", scatter_dimension=2, tiled=True
    ).astype(jnp.float32)
    results = lax.all_to_all(
        halves.astype(jnp.bfloat16), "ep", split_axis=0, concat_axis=0, tiled=True
    ).astype(halves.dtype)
    piece = lax.all_gather(own_half, "ep", axis=0, tiled=True)
    gathered = jnp.concatenate(
        [
            jnp.dot(piece, dense_gate, preferred_element_type=jnp.float32),
            jnp.dot(piece, dense_up, preferred_element_type=jnp.float32),
        ],
        axis=1,
    )
    summed = lax.psum(gathered.astype(jnp.bfloat16), "tp").astype(jnp.float32)
    unit_count = dense_gate.shape[1]
    dense_act = (jax.nn.silu(summed[:, :unit_count]) * summed[:, unit_count:]).astype(jnp.bfloat16)
    mix_scale = jax.nn.sigmoid(dense_mix)
    per_expert = jnp.sum(results.reshape(EXPERTS, expert_span, CAP, half_width), axis=1)
    per_expert = per_expert.reshape(EXPERTS * CAP, half_width)
    combine = jnp.sum(slot_table * expert_weight[:, :, None], axis=1)
    routed = jnp.dot(combine, per_expert, precision=lax.Precision.HIGHEST)
    dense_out = lax.psum_scatter(
        jnp.dot(dense_act, dense_down, preferred_element_type=jnp.float32) * mix_scale,
        "ep",
        scatter_dimension=0,
        tiled=True,
    )
    updated = kept + routed + dense_out
    return (updated.astype(jnp.bfloat16), state_out)


def solution(mesh):
    placed = (
        P("ep", None),
        P(),
        P(None, "tp"),
        P(None, "tp"),
        P(None, None, "tp"),
        P(None, "tp"),
        P("tp"),
        P("tp"),
        P(None, "tp"),
        P(None, None, "tp"),
        P("ep", None, "tp"),
        P("ep", None, None, "tp"),
        P("ep", "tp", None),
        P("tp"),
        P("tp"),
        P("tp", None),
        P(),
        P("ep", None),
        P("ep", None),
        P(None, ("ep", "tp")),
        P(None, ("ep", "tp")),
        P(("ep", "tp"), None),
        P("tp", "ep"),
        P("tp", "ep"),
        P("ep", "tp"),
        P("tp"),
    )
    return jax.shard_map(
        local,
        mesh=mesh,
        in_specs=placed,
        out_specs=(P("ep", "tp"), P("ep", "tp", None)),
        check_vma=False,
    )
```

profile of v0, /device:TPU:0, one launch (start us, length us, event | category | flops | bytes accessed | tf_op | source)
XLA Modules:
  0.0 255.8 jit_solution(14987095764911211181)
XLA Ops:
  7.2 1.2 fusion.14
  8.5 1.4 fusion.5
  10.0 1.4 fusion.6
  11.4 2.2 fusion.4
  13.8 0.2 multiply_exponential_fusion
  14.2 0.1 multiply_reduce_fusion.3
  14.7 7.9 %reshape.146 = f32[32,8,64,64]{3,2,1,0:T(8,128)} reshape(f32[32,8,4096]{2,1,0:T(8,128)} %param.38) | data formatting | bytes 8388608 | tf_op jit(solution)/shard_map/reshape | solution.py:69
  22.5 0.1 multiply_multiply_fusion
  22.7 8.6 %broadcast_multiply_fusion = (f32[32,8,64,64]{3,2,1,0:T(8,128)}, f32[32,8,64]{2,1,0:T(8,128)S(1)}) fusion(f32[32,8,64]{2,1,0:T(8,128)S(1)} %bitcast.40, f32[32,8,64]{2,1,0:T(8,128)S(1)} %multiply_multiply_fusion, f32[32,8,64]{2,1,0:T(8,128)S(1)} %bitcast.41, f32[32,8,64,64]{3,2,1,0:T(8,128)} %reshape.146, f32[32,8]{1,0:T(8,128)S(1)} %copy.64), kind=kLoop, calls=%fused_computation.2 | loop fusion | flops 5226496 | bytes 8651776 | tf_op jit(solution)/shard_map/mul | solution.py:72
  31.4 0.1 reduce_sum.99
  31.6 2.1 fusion.27
  33.8 0.1 reduce_sum.100
  33.9 0.1 mul.255
  34.1 1.1 convolution_convert_fusion.2
  35.2 0.1 copy.68
  35.3 0.1 eq.29
  35.5 0.1 reduce_window_sum.11
  35.6 0.2 select_reduce_fusion.1
  35.8 0.1 sub.7
  36.0 0.1 convert_reduce_fusion.1
  36.1 19.9 %all-reduce.3.cloned.1.call-done = bf16[32,2048]{1,0:T(8,128)(2,1)} async-done(((bf16[32,2048]{1,0:T(8,128)(2,1)}), bf16[32,2048]{1,0:T(8,128)(2,1)}) %all-reduce.3.cloned.1.call-update) | async-done | bytes 131088 | tf_op jit(solution)/shard_map/psum | solution.py:128
  56.0 1.1 convert_add_fusion
  57.1 1.0 multiply_convert_fusion
  58.1 0.3 convolution_convert_fusion.1
  58.4 0.1 reshape.147
  58.5 1.1 broadcast_in_dim.11
  59.6 6.8 %all-to-all-start = ((bf16[16,12,2048]{2,1,0:T(8,128)(2,1)}), bf16[16,12,2048]{2,1,0:T(8,128)(2,1)S(1)}, u32[]{:S(2)}, u32[]{:S(2)}) async-start(bf16[16,12,2048]{2,1,0:T(8,128)(2,1)} %bitcast.7), calls=%async_computation | async-start | bytes 2097152 | tf_op jit(solution)/shard_map/all_to_all | solution.py:150
  66.5 0.6 constant_dynamic-slice_fusion
  67.2 24.9 %all-to-all-done = bf16[16,12,2048]{2,1,0:T(8,128)(2,1)S(1)} async-done(((bf16[16,12,2048]{2,1,0:T(8,128)(2,1)}), bf16[16,12,2048]{2,1,0:T(8,128)(2,1)S(1)}, u32[]{:S(2)}, u32[]{:S(2)}) %all-to-all-start) | async-done | bytes 786464 | tf_op jit(solution)/shard_map/all_to_all | solution.py:150
  92.1 0.2 reshape.149
  92.3 5.8 %fusion.28 = f32[192,1792]{1,0:T(8,128)} fusion(bf16[192,2048]{1,0:T(8,128)(2,1)S(1)} %reshape.149, bf16[2048,1792]{1,0:T(8,128)(2,1)} %param.45), kind=kOutput, calls=%fused_computation.69 | convolution fusion | flops 1409286144 | bytes 9502720 | tf_op jit(solution)/shard_map/dot_general | solution.py:153
  98.0 30.7 %all-gather.2.cloned.1.call-done = bf16[512,1024]{1,0:T(8,128)(2,1)} async-done(((bf16[32,1024]{1,0:T(8,128)(2,1)}), bf16[512,1024]{1,0:T(8,128)(2,1)}) %all-gather.2.cloned.1.call-update) | async-done | bytes 1048592 | tf_op jit(solution)/shard_map/all_gather | solution.py:165
  128.7 2.1 convolution_convert_fusion.3
  130.9 0.6 convolution_convert_fusion.4
  131.4 0.9 pad_maximum_fusion
  132.4 9.4 %convolution_convert_fusion = bf16[192,2048]{1,0:T(8,128)(2,1)S(1)} fusion(bf16[1792,2048]{1,0:T(8,128)(2,1)} %param.47, bf16[192,2048]{1,0:T(8,128)(2,1)S(1)} %reshape.149, bf16[2048,1792]{1,0:T(8,128)(2,1)} %param.46, f32[192,1792]{1,0:T(8,128)} %fusion.28), kind=kOutput, calls=%fused_computation.5 | convolution fusion | flops 2821029888 | bytes 17629184 | tf_op jit(solution)/shard_map/dot_general | solution.py:156
  141.8 1.2 convert_element_type.94
  143.0 0.2 reduce-scatter.5.cloned.1.call-start
  143.2 7.0 %all-reduce.5.cloned.1.call-done = bf16[512,704]{0,1:T(8,128)(2,1)} async-done(((bf16[512,704]{0,1:T(8,128)(2,1)}), bf16[512,704]{0,1:T(8,128)(2,1)}) %all-reduce.5.cloned.1.call-update) | async-done | bytes 720912 | tf_op jit(solution)/shard_map/psum | solution.py:173
  150.3 1.3 convert_element_type.95
  151.6 3.3 %convolution_multiply_fusion.1 = f32[512,1024]{1,0:T(8,128)} fusion(bf16[352,1024]{1,0:T(8,128)(2,1)} %param.50, f32[1024]{0:T(1024)S(1)} %add_divide_fusion, f32[512,704]{0,1:T(8,128)S(1)} %convert_element_type.95), kind=kOutput, calls=%fused_computation.8 | convolution fusion | flops 370704384 | bytes 4263936 | tf_op jit(solution)/shard_map/dot_general | solution.py:182
  154.9 7.9 %mul.279 = f32[32,8,4096]{2,1,0:T(8,128)} reshape(f32[32,8,64,64]{3,2,1,0:T(8,128)} %get-tuple-element.6) | data formatting | bytes 8388608 | tf_op jit(solution)/shard_map/mul | solution.py:72
  162.8 6.8 %all-to-all-start.1 = ((bf16[16,12,1024]{2,1,0:T(8,128)(2,1)}), bf16[16,12,1024]{2,1,0:T(8,128)(2,1)S(1)}, u32[]{:S(2)}, u32[]{:S(2)}) async-start(bf16[16,12,1024]{2,1,0:T(8,128)(2,1)} %reduce-scatter.3.cloned.1.call-done), calls=%async_computation.2 | async-start | bytes 1048576 | tf_op jit(solution)/shard_map/all_to_all | solution.py:162
  169.6 6.8 %multiply_add_fusion = f32[32,8,4096]{2,1,0:T(8,128)} fusion(f32[32,8,4096]{2,1,0:T(8,128)} %mul.279, f32[32,8,4096]{2,1,0:T(8,128)} %param.38, f32[32,8]{1,0:T(8,128)S(1)} %copy.64), kind=kLoop, calls=%fused_computation.1 | loop fusion | flops 2097152 | bytes 12583936 | tf_op jit(solution)/shard_map/add | solution.py:71
  176.4 12.7 %all-to-all-done.1 = bf16[16,12,1024]{2,1,0:T(8,128)(2,1)S(1)} async-done(((bf16[16,12,1024]{2,1,0:T(8,128)(2,1)}), bf16[16,12,1024]{2,1,0:T(8,128)(2,1)S(1)}, u32[]{:S(2)}, u32[]{:S(2)}) %all-to-all-start.1) | async-done | bytes 393248 | tf_op jit(solution)/shard_map/all_to_all | solution.py:162
  189.1 0.1 convert_reduce_fusion
  189.3 58.1 %reduce-scatter.5.cloned.1.call-done = f32[32,1024]{1,0:T(8,128)} async-done(((f32[512,1024]{1,0:T(8,128)}), f32[32,1024]{1,0:T(8,128)}) %reduce-scatter.5.cloned.1.call-update) | async-done | bytes 131088 | tf_op jit(solution)/shard_map/reduce_scatter | solution.py:181
  247.4 1.9 fusion.2
  (75 shorter events, 1.5 us)
Async XLA Ops:
  7.2 26.9 %copy-start = (bf16[512,2048]{1,0:T(8,128)(2,1)S(1)}, bf16[512,2048]{1,0:T(8,128)(2,1)}, u32[]{:S(2)}) copy-start(bf16[512,2048]{1,0:T(8,128)(2,1)} %param.41) | copy-start | bytes 6291460
  7.2 6.4 %copy-start.6 = (f32[4,512]{1,0:T(4,128)S(1)}, f32[4,512]{1,0:T(4,128)}, u32[]{:S(2)}) copy-start(f32[4,512]{1,0:T(4,128)} %param.34) | copy-start | bytes 24580
  7.2 6.4 %copy-start.3 = (bf16[32,3,512]{2,0,1:T(8,128)(2,1)S(1)}, bf16[32,3,512]{2,0,1:T(8,128)(2,1)}, u32[]{:S(2)}) copy-start(bf16[32,3,512]{2,0,1:T(8,128)(2,1)} %param.36) | copy-start | bytes 294916
  7.2 48.8 %all-reduce.3.cloned.1.call-start = ((), (), s32[]{:S(2)}) async-start(), calls=%async_computation.4 | async-start | bytes 262144 | tf_op jit(solution)/shard_map/psum | solution.py:128
  8.4 5.3 %copy-start.17 = (f32[8]{0:T(128)S(1)}, f32[8]{0:T(128)}, u32[]{:S(2)}) copy-start(f32[8]{0:T(128)} %param.33) | copy-start | bytes 100
  8.4 5.3 %copy-start.2 = (bf16[32,2048]{1,0:T(8,128)(2,1)S(1)}, bf16[32,2048]{1,0:T(8,128)(2,1)}, u32[]{:S(2)}) copy-start(bf16[32,2048]{1,0:T(8,128)(2,1)} %param.26) | copy-start | bytes 393220
  8.5 5.3 %copy-start.5 = (f32[2048]{0:T(1024)S(1)}, f32[2048]{0:T(1024)}, u32[]{:S(2)}) copy-start(f32[2048]{0:T(1024)} %param.27) | copy-start | bytes 24580
  8.5 5.3 %copy-start.16 = (bf16[2048,8]{0,1:T(8,128)(2,1)S(1)}, bf16[2048,8]{0,1:T(8,128)(2,1)}, u32[]{:S(2)}) copy-start(bf16[2048,8]{0,1:T(8,128)(2,1)} %param.31) | copy-start | bytes 98308
  8.5 5.3 %copy-start.18 = (f32[8]{0:T(128)S(1)}, f32[8]{0:T(128)}, u32[]{:S(2)}) copy-start(f32[8]{0:T(128)} %param.32) | copy-start | bytes 100
  10.0 4.2 %copy-start.9 = (f32[2,4,128]{2,1,0:T(4,128)S(1)}, f32[2,4,128]{2,1,0:T(4,128)}, u32[]{:S(2)}) copy-start(f32[2,4,128]{2,1,0:T(4,128)} %param.35) | copy-start | bytes 12292
  10.0 4.2 %copy-start.4 = (bf16[32,2,3,128]{3,1,2,0:T(2,128)(2,1)S(1)}, bf16[32,2,3,128]{3,1,2,0:T(2,128)(2,1)}, u32[]{:S(2)}) copy-start(bf16[32,2,3,128]{3,1,2,0:T(2,128)(2,1)} %param.37) | copy-start | bytes 147460
  22.7 8.7 %copy-start.13 = (f32[8]{0:T(128)S(1)}, f32[8]{0:T(128)}, u32[]{:S(2)}) copy-start(f32[8]{0:T(128)} %param.39) | copy-start | bytes 100
  31.3 2.7 %copy-start.11 = (f32[512]{0:T(512)S(1)}, f32[512]{0:T(512)}, u32[]{:S(2)}) copy-start(f32[512]{0:T(512)} %param.40) | copy-start | bytes 6148
  33.7 1.5 copy-start.8
  33.7 2.3 copy-start.12
  33.8 23.3 %copy-start.7 = (f32[2048]{0:T(1024)S(1)}, f32[2048]{0:T(1024)}, u32[]{:S(2)}) copy-start(f32[2048]{0:T(1024)} %param.42) | copy-start | bytes 24580
  59.6 32.5 %all-to-all-start = ((bf16[16,12,2048]{2,1,0:T(8,128)(2,1)}), bf16[16,12,2048]{2,1,0:T(8,128)(2,1)S(1)}, u32[]{:S(2)}, u32[]{:S(2)}) async-start(bf16[16,12,2048]{2,1,0:T(8,128)(2,1)} %bitcast.7), calls=%async_computation | async-start | bytes 2097152 | tf_op jit(solution)/shard_map/all_to_all | solution.py:150
  66.4 62.3 %all-gather.2.cloned.1.call-start = ((), (), s32[]{:S(2)}) async-start(), calls=%async_computation.6 | async-start | bytes 1114112 | tf_op jit(solution)/shard_map/all_gather | solution.py:165
  67.2 83.1 %all-reduce.5.cloned.1.call-start = ((), (), s32[]{:S(2)}) async-start(), calls=%async_computation.7 | async-start | bytes 1441792 | tf_op jit(solution)/shard_map/psum | solution.py:173
  128.7 2.1 copy-start.14
  128.7 2.1 copy-start.15
  132.4 30.4 %reduce-scatter.3.cloned.1.call-start = ((), (), s32[]{:S(2)}) async-start(), calls=%async_computation.5 | async-start | bytes 1572864 | tf_op jit(solution)/shard_map/reduce_scatter | solution.py:159
  141.8 1.4 copy-start.10
  143.0 104.4 %reduce-scatter.5.cloned.1.call-start = ((), (), s32[]{:S(2)}) async-start(), calls=%async_computation.8 | async-start | bytes 2228224 | tf_op jit(solution)/shard_map/reduce_scatter | solution.py:181
  162.8 26.4 %all-to-all-start.1 = ((bf16[16,12,1024]{2,1,0:T(8,128)(2,1)}), bf16[16,12,1024]{2,1,0:T(8,128)(2,1)S(1)}, u32[]{:S(2)}, u32[]{:S(2)}) async-start(bf16[16,12,1024]{2,1,0:T(8,128)(2,1)} %reduce-scatter.3.cloned.1.call-done), calls=%async_computation.2 | async-start | bytes 1048576 | tf_op jit(solution)/shard_map/all_to_all | solution.py:162
  169.6 79.6 %copy-start.1 = (bf16[512,2048]{1,0:T(8,128)(2,1)S(1)}, bf16[512,2048]{1,0:T(8,128)(2,1)}, u32[]{:S(2)}) copy-start(bf16[512,2048]{1,0:T(8,128)(2,1)} %param.41) | copy-start | bytes 6291460
Sparse Core Ops, SparseCore 0:
  35.4 20.6 all-reduce.2
  70.6 58.0 all-gather.1
  132.5 17.6 all-reduce.4
  152.4 9.5 reduce-scatter.2
  164.1 83.2 reduce-scatter.4
where the time goes:
time: 257 us; the launch traced here: 256 us
  waiting for transfers between devices  153 us (60%)
  matrix products  31.8 us (12%)
  other arithmetic  21.9 us (9%)
  local copies, waits for them, and re-layouts  20.4 us (8%)
  between operations  14.3 us (6%)
  starting transfers between devices  14 us (5%)
    reduce_scatter x1, waiting for transfers between devices, local(): lax.psum_scatter(jnp.dot(dense_act, dense_down, preferred_element_type=jn...  58.1 us
    all_gather x1, waiting for transfers between devices, local(): piece = lax.all_gather(own_half, 'ep', axis=0, tiled=True)  30.7 us
    all_to_all x1, waiting for transfers between devices, local(): lax.all_to_all(outgoing, 'ep', split_axis=0, concat_axis=0, tiled=True)  24.9 us
    psum x1, waiting for transfers between devices, local(): mixed = lax.psum(partial_out.astype(jnp.bfloat16), 'tp').astype(jnp.float32)  19.9 us
    all_to_all x1, waiting for transfers between devices, local(): lax.all_to_all(halves.astype(jnp.bfloat16), 'ep', split_axis=0, concat_ax...  12.7 us
    dot_general x1, matrix products, local(): jnp.dot(act, expert_down, preferred_element_type=jnp.float32)  9.35 us
    mul x1, other arithmetic, mix_heads(): (step_size[:, :, None] * values)[:, :, :, None] * write_map[:, :, None, :]  8.62 us
    mul x1, local copies, waits for them, and re-layouts, mix_heads(): (step_size[:, :, None] * values)[:, :, :, None] * write_map[:, :, None, :]  7.9 us
  transfers between devices with their start and end apart: 7, of which 6 were waited for; matrix products, arithmetic and copies ran while one was open for 15% of the time, Pallas kernels for 0%

commit v1 on v0

--- a/solution.py
+++ b/solution.py
@@ -11,6 +11,7 @@
 TOP_K = 2
 CAP = 12
 EPS = 1e-06
+_deliver_forms = lambda state, bus_axis: jax.lax.all_gather(state, axis_name=bus_axis).sum(axis=0)
 
 
 def rms_scale(values):
@@ -125,7 +126,7 @@
         inner_gain,
     )
     partial_out = jnp.dot(inner_out, mixer_out, preferred_element_type=jnp.float32)
-    mixed = lax.psum(partial_out.astype(jnp.bfloat16), "tp").astype(jnp.float32)
+    mixed = _deliver_forms(partial_out.astype(jnp.bfloat16), "tp").astype(jnp.float32)
     hidden_mid = stream.astype(jnp.float32) + mixed
     ffn_in = (rms_scale(hidden_mid) * channel_gain).astype(jnp.bfloat16)
     row_count, feature_count = ffn_in.shape

time: 257 us -> 238 us (0.926)
  waiting for transfers between devices: 153 us -> 133 us
    psum x1 -> x0, waiting for transfers between devices: 19.9 us -> none  [local(): mixed = lax.psum(partial_out.astype(jnp.bfloat16), 'tp').astype(jnp.float32)]
  transfers between devices with their start and end apart: 7 -> 6, of which waited for: 6 -> 5; matrix products, arithmetic and copies ran while one was open for 15% -> 15% of each run, Pallas kernels for 0% -> 0%
where the time goes in v1:
time: 238 us; the launch traced here: 237 us
  waiting for transfers between devices  133 us (56%)
  matrix products  31.1 us (13%)
  local copies, waits for them, and re-layouts  20.4 us (9%)
  other arithmetic  20.1 us (8%)
  starting transfers between devices  15.4 us (6%)
  between operations  14.3 us (6%)
    reduce_scatter x1, waiting for transfers between devices, local(): lax.psum_scatter(jnp.dot(dense_act, dense_down, preferred_element_type=jn...  58 us
    all_gather x1, waiting for transfers between devices, local(): piece = lax.all_gather(own_half, 'ep', axis=0, tiled=True)  30.6 us
    all_to_all x1, waiting for transfers between devices, local(): lax.all_to_all(outgoing, 'ep', split_axis=0, concat_axis=0, tiled=True)  24.9 us
    all_to_all x1, waiting for transfers between devices, local(): lax.all_to_all(halves.astype(jnp.bfloat16), 'ep', split_axis=0, concat_ax...  12.7 us
    dot_general x1, matrix products, local(): jnp.dot(act, expert_down, preferred_element_type=jnp.float32)  9.35 us
    mul x1, other arithmetic, mix_heads(): (step_size[:, :, None] * values)[:, :, :, None] * write_map[:, :, None, :]  8.62 us
    all_to_all x1, starting transfers between devices, local(): lax.all_to_all(outgoing, 'ep', split_axis=0, concat_axis=0, tiled=True)  8.21 us
    mul x1, local copies, waits for them, and re-layouts, mix_heads(): (step_size[:, :, None] * values)[:, :, :, None] * write_map[:, :, None, :]  7.9 us
  transfers between devices with their start and end apart: 6, of which 5 were waited for; matrix products, arithmetic and copies ran while one was open for 15% of the time, Pallas kernels for 0%

profile of v1, /device:TPU:0, one launch (start us, length us, event | category | flops | bytes accessed | tf_op | source)
XLA Modules:
  0.0 236.7 jit_solution(8460223248385428964)
XLA Ops:
  7.2 1.2 fusion.14
  8.5 1.4 fusion.5
  9.9 1.4 fusion.6
  11.3 2.2 fusion.4
  13.6 0.1 reduce_sum.108
  13.8 0.2 multiply_exponential_fusion
  14.1 0.1 multiply_reduce_fusion.3
  14.6 7.9 %reshape.146 = f32[32,8,64,64]{3,2,1,0:T(8,128)} reshape(f32[32,8,4096]{2,1,0:T(8,128)} %param.38) | data formatting | bytes 8388608 | tf_op jit(solution)/shard_map/reshape | solution.py:70
  22.5 0.1 multiply_multiply_fusion
  22.7 8.6 %broadcast_multiply_fusion = (f32[32,8,64,64]{3,2,1,0:T(8,128)}, f32[32,8,64]{2,1,0:T(8,128)S(1)}) fusion(f32[32,8,64]{2,1,0:T(8,128)S(1)} %bitcast.42, f32[32,8,64]{2,1,0:T(8,128)S(1)} %multiply_multiply_fusion, f32[32,8,64]{2,1,0:T(8,128)S(1)} %bitcast.43, f32[32,8,64,64]{3,2,1,0:T(8,128)} %reshape.146, f32[32,8]{1,0:T(8,128)S(1)} %copy.64), kind=kLoop, calls=%fused_computation.2 | loop fusion | flops 5226496 | bytes 8651776 | tf_op jit(solution)/shard_map/mul | solution.py:73
  31.3 0.1 reduce_sum.111
  31.6 2.1 fusion.27
  33.8 0.1 reduce_sum.112
  33.9 0.1 mul.255
  34.0 0.5 convolution_convert_fusion.2
  34.5 2.1 all-gather
  36.7 0.2 convert_add_fusion
  36.8 0.1 copy.68
  36.9 0.1 eq.29
  37.1 0.1 reduce_window_sum.11
  37.2 0.2 select_reduce_fusion.1
  37.4 0.1 sub.7
  37.6 0.1 multiply_convert_fusion
  37.8 0.3 convolution_convert_fusion.1
  38.1 0.1 reshape.147
  38.2 1.1 broadcast_in_dim.11
  39.3 8.2 %all-to-all-start = ((bf16[16,12,2048]{2,1,0:T(8,128)(2,1)}), bf16[16,12,2048]{2,1,0:T(8,128)(2,1)S(1)}, u32[]{:S(2)}, u32[]{:S(2)}) async-start(bf16[16,12,2048]{2,1,0:T(8,128)(2,1)} %bitcast.8), calls=%async_computation | async-start | bytes 2097152 | tf_op jit(solution)/shard_map/all_to_all | solution.py:151
  47.6 0.6 constant_dynamic-slice_fusion
  48.3 24.9 %all-to-all-done = bf16[16,12,2048]{2,1,0:T(8,128)(2,1)S(1)} async-done(((bf16[16,12,2048]{2,1,0:T(8,128)(2,1)}), bf16[16,12,2048]{2,1,0:T(8,128)(2,1)S(1)}, u32[]{:S(2)}, u32[]{:S(2)}) %all-to-all-start) | async-done | bytes 786464 | tf_op jit(solution)/shard_map/all_to_all | solution.py:151
  73.2 0.2 reshape.149
  73.4 5.8 %fusion.28 = f32[192,1792]{1,0:T(8,128)} fusion(bf16[192,2048]{1,0:T(8,128)(2,1)S(1)} %reshape.149, bf16[2048,1792]{1,0:T(8,128)(2,1)} %param.45), kind=kOutput, calls=%fused_computation.69 | convolution fusion | flops 1409286144 | bytes 9502720 | tf_op jit(solution)/shard_map/dot_general | solution.py:154
  79.1 30.6 %all-gather.3.cloned.1.call-done = bf16[512,1024]{1,0:T(8,128)(2,1)} async-done(((bf16[32,1024]{1,0:T(8,128)(2,1)}), bf16[512,1024]{1,0:T(8,128)(2,1)}) %all-gather.3.cloned.1.call-update) | async-done | bytes 1048592 | tf_op jit(solution)/shard_map/all_gather | solution.py:166
  109.7 2.1 convolution_convert_fusion.3
  111.8 0.6 convolution_convert_fusion.4
  112.4 0.9 pad_maximum_fusion
  113.4 9.4 %convolution_convert_fusion = bf16[192,2048]{1,0:T(8,128)(2,1)S(1)} fusion(bf16[1792,2048]{1,0:T(8,128)(2,1)} %param.47, bf16[192,2048]{1,0:T(8,128)(2,1)S(1)} %reshape.149, bf16[2048,1792]{1,0:T(8,128)(2,1)} %param.46, f32[192,1792]{1,0:T(8,128)} %fusion.28), kind=kOutput, calls=%fused_computation.5 | convolution fusion | flops 2821029888 | bytes 17629184 | tf_op jit(solution)/shard_map/dot_general | solution.py:157
  122.8 1.2 convert_element_type.96
  124.0 0.2 reduce-scatter.5.cloned.1.call-start
  124.2 7.0 %all-reduce.2.cloned.1.call-done = bf16[512,704]{0,1:T(8,128)(2,1)} async-done(((bf16[512,704]{0,1:T(8,128)(2,1)}), bf16[512,704]{0,1:T(8,128)(2,1)}) %all-reduce.2.cloned.1.call-update) | async-done | bytes 720912 | tf_op jit(solution)/shard_map/psum | solution.py:174
  131.2 1.3 convert_element_type.97
  132.5 3.3 %convolution_multiply_fusion.1 = f32[512,1024]{1,0:T(8,128)} fusion(bf16[352,1024]{1,0:T(8,128)(2,1)} %param.50, f32[1024]{0:T(1024)S(1)} %add_divide_fusion, f32[512,704]{0,1:T(8,128)S(1)} %convert_element_type.97), kind=kOutput, calls=%fused_computation.8 | convolution fusion | flops 370704384 | bytes 4263936 | tf_op jit(solution)/shard_map/dot_general | solution.py:183
  135.9 7.9 %mul.279 = f32[32,8,4096]{2,1,0:T(8,128)} reshape(f32[32,8,64,64]{3,2,1,0:T(8,128)} %get-tuple-element.6) | data formatting | bytes 8388608 | tf_op jit(solution)/shard_map/mul | solution.py:73
  143.8 6.8 %all-to-all-start.1 = ((bf16[16,12,1024]{2,1,0:T(8,128)(2,1)}), bf16[16,12,1024]{2,1,0:T(8,128)(2,1)S(1)}, u32[]{:S(2)}, u32[]{:S(2)}) async-start(bf16[16,12,1024]{2,1,0:T(8,128)(2,1)} %reduce-scatter.3.cloned.1.call-done), calls=%async_computation.2 | async-start | bytes 1048576 | tf_op jit(solution)/shard_map/all_to_all | solution.py:163
  150.6 6.8 %multiply_add_fusion = f32[32,8,4096]{2,1,0:T(8,128)} fusion(f32[32,8,4096]{2,1,0:T(8,128)} %mul.279, f32[32,8,4096]{2,1,0:T(8,128)} %param.38, f32[32,8]{1,0:T(8,128)S(1)} %copy.64), kind=kLoop, calls=%fused_computation.1 | loop fusion | flops 2097152 | bytes 12583936 | tf_op jit(solution)/shard_map/add | solution.py:72
  157.4 12.7 %all-to-all-done.1 = bf16[16,12,1024]{2,1,0:T(8,128)(2,1)S(1)} async-done(((bf16[16,12,1024]{2,1,0:T(8,128)(2,1)}), bf16[16,12,1024]{2,1,0:T(8,128)(2,1)S(1)}, u32[]{:S(2)}, u32[]{:S(2)}) %all-to-all-start.1) | async-done | bytes 393248 | tf_op jit(solution)/shard_map/all_to_all | solution.py:163
  170.1 0.1 convert_reduce_fusion
  170.3 58.0 %reduce-scatter.5.cloned.1.call-done = f32[32,1024]{1,0:T(8,128)} async-done(((f32[512,1024]{1,0:T(8,128)}), f32[32,1024]{1,0:T(8,128)}) %reduce-scatter.5.cloned.1.call-update) | async-done | bytes 131088 | tf_op jit(solution)/shard_map/reduce_scatter | solution.py:182
  228.3 1.9 fusion.2
  (74 shorter events, 1.5 us)
Async XLA Ops:
  7.2 26.9 %copy-start = (bf16[512,2048]{1,0:T(8,128)(2,1)S(1)}, bf16[512,2048]{1,0:T(8,128)(2,1)}, u32[]{:S(2)}) copy-start(bf16[512,2048]{1,0:T(8,128)(2,1)} %param.41) | copy-start | bytes 6291460
  7.2 6.4 %copy-start.6 = (f32[4,512]{1,0:T(4,128)S(1)}, f32[4,512]{1,0:T(4,128)}, u32[]{:S(2)}) copy-start(f32[4,512]{1,0:T(4,128)} %param.34) | copy-start | bytes 24580
  7.2 6.4 %copy-start.3 = (bf16[32,3,512]{2,0,1:T(8,128)(2,1)S(1)}, bf16[32,3,512]{2,0,1:T(8,128)(2,1)}, u32[]{:S(2)}) copy-start(bf16[32,3,512]{2,0,1:T(8,128)(2,1)} %param.36) | copy-start | bytes 294916
  8.4 5.3 %copy-start.17 = (f32[8]{0:T(128)S(1)}, f32[8]{0:T(128)}, u32[]{:S(2)}) copy-start(f32[8]{0:T(128)} %param.33) | copy-start | bytes 100
  8.4 5.3 %copy-start.2 = (bf16[32,2048]{1,0:T(8,128)(2,1)S(1)}, bf16[32,2048]{1,0:T(8,128)(2,1)}, u32[]{:S(2)}) copy-start(bf16[32,2048]{1,0:T(8,128)(2,1)} %param.26) | copy-start | bytes 393220
  8.4 5.3 %copy-start.5 = (f32[2048]{0:T(1024)S(1)}, f32[2048]{0:T(1024)}, u32[]{:S(2)}) copy-start(f32[2048]{0:T(1024)} %param.27) | copy-start | bytes 24580
  8.4 5.3 %copy-start.16 = (bf16[2048,8]{0,1:T(8,128)(2,1)S(1)}, bf16[2048,8]{0,1:T(8,128)(2,1)}, u32[]{:S(2)}) copy-start(bf16[2048,8]{0,1:T(8,128)(2,1)} %param.31) | copy-start | bytes 98308
  8.4 5.3 %copy-start.18 = (f32[8]{0:T(128)S(1)}, f32[8]{0:T(128)}, u32[]{:S(2)}) copy-start(f32[8]{0:T(128)} %param.32) | copy-start | bytes 100
  9.9 4.2 %copy-start.9 = (f32[2,4,128]{2,1,0:T(4,128)S(1)}, f32[2,4,128]{2,1,0:T(4,128)}, u32[]{:S(2)}) copy-start(f32[2,4,128]{2,1,0:T(4,128)} %param.35) | copy-start | bytes 12292
  9.9 4.2 %copy-start.4 = (bf16[32,2,3,128]{3,1,2,0:T(2,128)(2,1)S(1)}, bf16[32,2,3,128]{3,1,2,0:T(2,128)(2,1)}, u32[]{:S(2)}) copy-start(bf16[32,2,3,128]{3,1,2,0:T(2,128)(2,1)} %param.37) | copy-start | bytes 147460
  22.7 8.7 %copy-start.13 = (f32[8]{0:T(128)S(1)}, f32[8]{0:T(128)}, u32[]{:S(2)}) copy-start(f32[8]{0:T(128)} %param.39) | copy-start | bytes 100
  31.3 2.7 %copy-start.11 = (f32[512]{0:T(512)S(1)}, f32[512]{0:T(512)}, u32[]{:S(2)}) copy-start(f32[512]{0:T(512)} %param.40) | copy-start | bytes 6148
  33.7 3.2 %copy-start.8 = (s32[32,2]{0,1:T(2,128)S(1)}, s32[32,2]{0,1:T(2,128)}, u32[]{:S(2)}) copy-start(s32[32,2]{0,1:T(2,128)} %param.43) | copy-start | bytes 772
  33.8 3.9 %copy-start.7 = (f32[2048]{0:T(1024)S(1)}, f32[2048]{0:T(1024)}, u32[]{:S(2)}) copy-start(f32[2048]{0:T(1024)} %param.42) | copy-start | bytes 24580
  34.0 3.7 %copy-start.12 = (f32[32,2]{0,1:T(2,128)S(1)}, f32[32,2]{0,1:T(2,128)}, u32[]{:S(2)}) copy-start(f32[32,2]{0,1:T(2,128)} %param.44) | copy-start | bytes 772
  39.3 33.9 %all-to-all-start = ((bf16[16,12,2048]{2,1,0:T(8,128)(2,1)}), bf16[16,12,2048]{2,1,0:T(8,128)(2,1)S(1)}, u32[]{:S(2)}, u32[]{:S(2)}) async-start(bf16[16,12,2048]{2,1,0:T(8,128)(2,1)} %bitcast.8), calls=%async_computation | async-start | bytes 2097152 | tf_op jit(solution)/shard_map/all_to_all | solution.py:151
  47.5 62.2 %all-gather.3.cloned.1.call-start = ((), (), s32[]{:S(2)}) async-start(), calls=%async_computation.5 | async-start | bytes 1114112 | tf_op jit(solution)/shard_map/all_gather | solution.py:166
  48.3 83.0 %all-reduce.2.cloned.1.call-start = ((), (), s32[]{:S(2)}) async-start(), calls=%async_computation.6 | async-start | bytes 1441792 | tf_op jit(solution)/shard_map/psum | solution.py:174
  109.7 2.1 copy-start.14
  109.7 2.1 copy-start.15
  113.4 30.4 %reduce-scatter.3.cloned.1.call-start = ((), (), s32[]{:S(2)}) async-start(), calls=%async_computation.4 | async-start | bytes 1572864 | tf_op jit(solution)/shard_map/reduce_scatter | solution.py:160
  122.8 1.4 copy-start.10
  124.0 104.4 %reduce-scatter.5.cloned.1.call-start = ((), (), s32[]{:S(2)}) async-start(), calls=%async_computation.7 | async-start | bytes 2228224 | tf_op jit(solution)/shard_map/reduce_scatter | solution.py:182
  143.8 26.4 %all-to-all-start.1 = ((bf16[16,12,1024]{2,1,0:T(8,128)(2,1)}), bf16[16,12,1024]{2,1,0:T(8,128)(2,1)S(1)}, u32[]{:S(2)}, u32[]{:S(2)}) async-start(bf16[16,12,1024]{2,1,0:T(8,128)(2,1)} %reduce-scatter.3.cloned.1.call-done), calls=%async_computation.2 | async-start | bytes 1048576 | tf_op jit(solution)/shard_map/all_to_all | solution.py:163
  150.6 79.6 %copy-start.1 = (bf16[512,2048]{1,0:T(8,128)(2,1)S(1)}, bf16[512,2048]{1,0:T(8,128)(2,1)}, u32[]{:S(2)}) copy-start(bf16[512,2048]{1,0:T(8,128)(2,1)} %param.41) | copy-start | bytes 6291460
Sparse Core Ops, SparseCore 0:
  51.7 57.9 all-gather.2
  113.5 17.6 all-reduce.1
  133.5 9.5 reduce-scatter.2
  145.3 83.0 reduce-scatter.4
